TPU v7x, 32 devices: a whole 2x2x4 slice. The times are simulated.
32 devices in a mesh: sp: 8 (over z, x), dp: 4 (over y, core).
Axes of the slice: x: 2, y: 2, z: 4, core: 2. Of those that a mesh axis runs over, the one named last changes fastest.
Arguments:
- residual_in: bfloat16 [4, 1024, 2048], P('dp', 'sp'), may hold values from -6 to 6
- query_proj: bfloat16 [4, 1024, 2048], P('dp', 'sp'), may hold values from -8 to 8
- key_proj: bfloat16 [4, 1024, 512], P('dp', 'sp'), may hold values from -8 to 8
- value_proj: bfloat16 [4, 1024, 512], P('dp', 'sp'), may hold values from -6 to 6
- query_gain: float32 [128], replicated, may hold values from 0.1 to 7
- key_gain: float32 [128], replicated, may hold values from 0.1 to 7
- out_weight: bfloat16 [2048, 2048], replicated, may hold values from -0.125 to 0.125
- post_gain: float32 [2048], replicated, may hold values from 0.1 to 1.9
- pre_gain: float32 [2048], replicated, may hold values from 0.1 to 1.9
- route_ids: int32 [4, 1024, 2], P('dp', 'sp'), may hold values from 0 to 31, as said below
- group_weight: float32 [4, 1024], P('dp', 'sp'), may hold values from 0.25 to 1
- first_share: float32 [4, 1024], P('dp', 'sp'), may hold values from 0.5 to 1
- gate_weight: bfloat16 [32, 2048, 512], P(('sp', 'dp')), may hold values from -0.125 to 0.125
- up_weight: bfloat16 [32, 2048, 512], P(('sp', 'dp')), may hold values from -0.125 to 0.125
- down_weight: bfloat16 [32, 512, 2048], P(('sp', 'dp')), may hold values from -0.25 to 0.25
Outputs:
- layer_out: bfloat16 [4, 1024, 2048], P('dp', 'sp')
Inputs may be any that keep to these rules, and one draw needn't show every extreme that they name: `route_ids`: each token names two different experts of one group of 8 consecutive experts. Among the 128 tokens of one device each group is chosen by exactly 32 tokens, no expert is named by more than 16 of them, and in every draw one expert of each group is named by exactly 16 tokens of every device.
All inputs are finite; a program needn't handle non-finite values.
Results may differ from a plain program's by a relative error of at most 0.009.
The roundings to bfloat16 on the way count: a program that leaves them out, or rounds other values in their place, can miss the bound.
Values may be sent and summed in bfloat16 or wider, within the bound.
A program may use at most 128 MiB of HBM per device.

v0:
```python
import jax
import jax.numpy as jnp
from jax import lax
from jax.sharding import PartitionSpec as P

HEADS = 16
KV_HEADS = 4
HEAD_DIM = 128
GRID_W = 64


EPSILON = 1e-06


def rotate_heads(raw_heads, gain_vec, positions):
    floats = raw_heads.astype(jnp.float32)
    normed = (
        floats * lax.rsqrt(jnp.mean(floats * floats, axis=-1, keepdims=True) + EPSILON) * gain_vec
    )
    quarter = raw_heads.shape[-1] // 4
    inverse = 10000.0 ** (-jnp.arange(quarter, dtype=jnp.float32) / quarter)
    grid_rows = (positions // GRID_W).astype(jnp.float32)[:, None] * inverse
    grid_cols = (positions % GRID_W).astype(jnp.float32)[:, None] * inverse
    angles = jnp.concatenate([grid_rows, grid_rows, grid_cols, grid_cols], axis=-1)[:, None, :]
    pieces = normed.reshape(normed.shape[:-1] + (2, 2, quarter))
    turned = jnp.stack([-pieces[..., 1, :], pieces[..., 0, :]], axis=-2).reshape(normed.shape)
    return (normed * jnp.cos(angles) + turned * jnp.sin(angles)).astype(jnp.bfloat16)


def attend_blocks(queries, keys_all, values_all):
    count_q, kv_count, group_size, head_width = queries.shape
    block = min(512, count_q)
    blocks = count_q // block
    scale = head_width ** (-0.5)
    zero_index = jnp.zeros((), jnp.int32)

    def one_item(item):
        which = item // kv_count
        head_index = item % kv_count
        start_row = which * block
        q_block = lax.dynamic_slice(
            queries,
            (start_row, head_index, zero_index, zero_index),
            (block, 1, group_size, head_width),
        )[:, 0]
        key_block = lax.dynamic_slice(
            keys_all, (zero_index, head_index, zero_index), (keys_all.shape[0], 1, head_width)
        )[:, 0]
        value_block = lax.dynamic_slice(
            values_all, (zero_index, head_index, zero_index), (values_all.shape[0], 1, head_width)
        )[:, 0]
        scores = (
            jnp.einsum("qgd,sd->gqs", q_block, key_block, preferred_element_type=jnp.float32)
            * scale
        )
        shifted = jnp.exp(scores - jnp.max(scores, axis=-1, keepdims=True))
        weights = (shifted / jnp.sum(shifted, axis=-1, keepdims=True)).astype(jnp.bfloat16)
        return jnp.einsum(
            "gqs,sd->qgd", weights, value_block, preferred_element_type=jnp.float32
        ).astype(jnp.bfloat16)

    results = lax.map(one_item, jnp.arange(blocks * kv_count, dtype=jnp.int32))
    results = results.reshape(blocks, kv_count, block, group_size, head_width).transpose(
        0, 2, 1, 3, 4
    )
    return results.reshape(count_q, kv_count * group_size * head_width)


def rms_scale(values, gain_vec):
    floats = values.astype(jnp.float32)
    return (
        floats * lax.rsqrt(jnp.mean(floats * floats, axis=-1, keepdims=True) + EPSILON) * gain_vec
    )


def expert_ffn(arrived, gate_weight, up_weight, down_weight):
    gated = jnp.einsum("nesd,edf->nesf", arrived, gate_weight, preferred_element_type=jnp.float32)
    lifted = jnp.einsum("nesd,edf->nesf", arrived, up_weight, preferred_element_type=jnp.float32)
    hidden = (jax.nn.silu(gated) * lifted).astype(jnp.bfloat16)
    return jnp.einsum(
        "nesf,efd->nesd", hidden, down_weight, preferred_element_type=jnp.float32
    ).astype(jnp.bfloat16)


def local(
    residual_in,
    query_proj,
    key_proj,
    value_proj,
    query_gain,
    key_gain,
    out_weight,
    post_gain,
    pre_gain,
    route_ids,
    group_weight,
    first_share,
    gate_weight,
    up_weight,
    down_weight,
):
    sp_count = lax.axis_size("sp")
    dp_count = lax.axis_size("dp")
    tokens = query_proj.shape[1]
    group_size = HEADS // KV_HEADS
    key_all, value_all = (
        lax.all_gather(key_proj, "sp", axis=1, tiled=True),
        lax.all_gather(value_proj, "sp", axis=1, tiled=True),
    )
    length = key_all.shape[1]
    key_positions = jnp.arange(length, dtype=jnp.int32)
    query_positions = lax.axis_index("sp") * tokens + jnp.arange(tokens, dtype=jnp.int32)
    query_turned = rotate_heads(
        query_proj.reshape(tokens, HEADS, HEAD_DIM), query_gain, query_positions
    )
    key_turned = rotate_heads(key_all.reshape(length, KV_HEADS, HEAD_DIM), key_gain, key_positions)
    attended = attend_blocks(
        query_turned.reshape(tokens, KV_HEADS, group_size, HEAD_DIM),
        key_turned,
        value_all.reshape(length, KV_HEADS, HEAD_DIM),
    )
    mixed = jnp.dot(attended, out_weight, preferred_element_type=jnp.float32).astype(jnp.bfloat16)
    stream = (residual_in[0].astype(jnp.float32) + rms_scale(mixed, post_gain)).astype(jnp.bfloat16)
    normed = rms_scale(stream, pre_gain).astype(jnp.bfloat16)
    model_width = normed.shape[1]
    local_experts = gate_weight.shape[0]
    expert_count = local_experts * sp_count * dp_count
    capacity = 4 * tokens // expert_count
    chosen = route_ids.reshape(2 * tokens)
    onehot = (chosen[:, None] == jnp.arange(expert_count, dtype=jnp.int32)[None, :]).astype(
        jnp.int32
    )
    earlier = jnp.cumsum(onehot, axis=0) - onehot
    slot_rank = jnp.sum(earlier * onehot, axis=1)
    slot_index = chosen * capacity + slot_rank
    source_row = (
        jnp.full((expert_count * capacity,), tokens, jnp.int32)
        .at[slot_index]
        .set(jnp.arange(2 * tokens, dtype=jnp.int32) // 2)
    )
    padded = jnp.concatenate([normed, jnp.zeros((1, model_width), jnp.bfloat16)], axis=0)
    outgoing = padded[source_row]
    shaped = outgoing.reshape(sp_count * dp_count, local_experts, capacity, model_width)
    answered = expert_ffn(
        lax.all_to_all(shaped, ("sp", "dp"), split_axis=0, concat_axis=0, tiled=True),
        gate_weight,
        up_weight,
        down_weight,
    )
    returned = lax.all_to_all(answered, ("sp", "dp"), split_axis=0, concat_axis=0, tiled=True)
    results = (
        returned.reshape(expert_count * capacity, model_width)[slot_index]
        .astype(jnp.float32)
        .reshape(tokens, 2, model_width)
    )
    share = first_share[0]
    weight_pair = group_weight[0][:, None] * jnp.stack([share, 1.0 - share], axis=1)
    combined = jnp.sum(weight_pair[:, :, None] * results, axis=1)
    return (
        (stream.astype(jnp.float32) + combined).astype(jnp.bfloat16).reshape(1, tokens, model_width)
    )


def solution(mesh):
    placed = (
        P("dp", "sp", None),
        P("dp", "sp", None),
        P("dp", "sp", None),
        P("dp", "sp", None),
        P(),
        P(),
        P(),
        P(),
        P(),
        P("dp", "sp", None),
        P("dp", "sp"),
        P("dp", "sp"),
        P(("sp", "dp"), None, None),
        P(("sp", "dp"), None, None),
        P(("sp", "dp"), None, None),
    )
    return jax.shard_map(
        local, mesh=mesh, in_specs=placed, out_specs=P("dp", "sp", None), check_vma=False
    )
```

profile of v0, /device:TPU:0, one launch (start us, length us, event | category | flops | bytes accessed | tf_op | source)
XLA Modules:
  0.0 277.3 jit_solution(16013332365449823118)
XLA Ops:
  6.5 1.8 copy.34
  9.2 1.3 copy.35
  18.0 1.4 scatter_custom_fusion
  19.5 2.7 fusion.74
  24.8 26.7 %all-gather.5.cloned.1.call-done = bf16[1,1024,512]{1,2,0:T(8,128)(2,1)} async-done(((bf16[1,128,512]{1,2,0:T(8,128)(2,1)}), bf16[1,1024,512]{1,2,0:T(8,128)(2,1)}) %all-gather.5.cloned.1.call-update) | async-done | bytes 1048592 | tf_op jit(solution)/shard_map/all_gather | solution.py:107
  51.5 1.5 convert_element_type.177
  55.9 37.1 %all-gather.3.cloned.1.call-done = bf16[1,1024,512]{2,1,0:T(8,128)(2,1)} async-done(((bf16[1,128,512]{2,1,0:T(8,128)(2,1)}), bf16[1,1024,512]{2,1,0:T(8,128)(2,1)}) %all-gather.3.cloned.1.call-update) | async-done | bytes 1048592 | tf_op jit(solution)/shard_map/all_gather | solution.py:108
  93.0 2.3 copy.33
  95.3 37.3 %while.12 = (s32[]{:T(128)}, bf16[4,128,4,128]{1,3,2,0:T(8,128)(2,1)}, s32[4]{0:T(128)S(1)}, bf16[1024,4,128]{0,2,1:T(8,128)(2,1)}, bf16[1024,4,128]{0,2,1:T(8,1...) while((s32[]{:T(128)}, ...), condition=%wide.region_5.6_spmd, body=%wide.region_2.5_spmd.sunk | while | flops 273222144 | bytes 17569568 | solution.py:62
  97.5 1.4 fusion.110
  98.9 1.3 copy-done.1
  100.9 3.7 %fusion.112 = bf16[4,128,4,128]{1,3,2,0:T(8,128)(2,1)} fusion(bf16[4,128,4,128]{1,3,2,0:T(8,128)(2,1)} %get-tuple-element.176, s32[]{:T(128)} %get-tuple-element.175, f32[4,128]{1,0:T(4,128)S(1)} %fusion.111, bf16[1024,4,128]{0,2,1:T(8,128)(2,1)} %get-tuple-element.188, s32[]{:T(128)S(6)} %select_n.109, f32[1024,128,4]{1,0,2:T(8,128)} %copy-done.1), kind=kOutput, calls=%fused_computation.12.clone.1 | convolution fusion | flops 136906240 | bytes 4590084 | tf_op jit(solution)/shard_map/while/body/eval_jaxpr/gqs,sd->qgd/dot_general | solution.py:58
  106.9 1.4 fusion.110
  108.3 1.3 copy-done.1
  110.2 3.7 %fusion.112 = bf16[4,128,4,128]{1,3,2,0:T(8,128)(2,1)} fusion(bf16[4,128,4,128]{1,3,2,0:T(8,128)(2,1)} %get-tuple-element.176, s32[]{:T(128)} %get-tuple-element.175, f32[4,128]{1,0:T(4,128)S(1)} %fusion.111, bf16[1024,4,128]{0,2,1:T(8,128)(2,1)} %get-tuple-element.188, s32[]{:T(128)S(6)} %select_n.109, f32[1024,128,4]{1,0,2:T(8,128)} %copy-done.1), kind=kOutput, calls=%fused_computation.12.clone.1 | convolution fusion | flops 136906240 | bytes 4590084 | tf_op jit(solution)/shard_map/while/body/eval_jaxpr/gqs,sd->qgd/dot_general | solution.py:58
  116.2 1.4 fusion.110
  117.6 1.3 copy-done.1
  119.5 3.7 %fusion.112 = bf16[4,128,4,128]{1,3,2,0:T(8,128)(2,1)} fusion(bf16[4,128,4,128]{1,3,2,0:T(8,128)(2,1)} %get-tuple-element.176, s32[]{:T(128)} %get-tuple-element.175, f32[4,128]{1,0:T(4,128)S(1)} %fusion.111, bf16[1024,4,128]{0,2,1:T(8,128)(2,1)} %get-tuple-element.188, s32[]{:T(128)S(6)} %select_n.109, f32[1024,128,4]{1,0,2:T(8,128)} %copy-done.1), kind=kOutput, calls=%fused_computation.12.clone.1 | convolution fusion | flops 136906240 | bytes 4590084 | tf_op jit(solution)/shard_map/while/body/eval_jaxpr/gqs,sd->qgd/dot_general | solution.py:58
  125.5 1.4 fusion.110
  126.9 1.3 copy-done.1
  128.9 3.7 %fusion.112 = bf16[4,128,4,128]{1,3,2,0:T(8,128)(2,1)} fusion(bf16[4,128,4,128]{1,3,2,0:T(8,128)(2,1)} %get-tuple-element.176, s32[]{:T(128)} %get-tuple-element.175, f32[4,128]{1,0:T(4,128)S(1)} %fusion.111, bf16[1024,4,128]{0,2,1:T(8,128)(2,1)} %get-tuple-element.188, s32[]{:T(128)S(6)} %select_n.109, f32[1024,128,4]{1,0,2:T(8,128)} %copy-done.1), kind=kOutput, calls=%fused_computation.12.clone.1 | convolution fusion | flops 136906240 | bytes 4590084 | tf_op jit(solution)/shard_map/while/body/eval_jaxpr/gqs,sd->qgd/dot_general | solution.py:58
  132.6 5.0 %multiply_reduce_fusion.2 = (f32[128]{0:T(128)S(1)}, f32[128,2048]{1,0:T(8,128)S(1)}) fusion(bf16[128,2048]{0,1:T(8,128)(2,1)} %bitcast.191, bf16[2048,2048]{1,0:T(8,128)(2,1)} %param.23), kind=kOutput, calls=%fused_computation.60 | convolution fusion | flops 1074790272 | bytes 9961984 | tf_op jit(solution)/shard_map/dot_general | solution.py:122
  138.5 3.3 %gather_fusion = bf16[512,2048]{1,0:T(8,128)(2,1)} fusion(bf16[129,2048]{1,0:T(8,128)(2,1)S(1)} %concatenate.31, s32[1024]{0:T(1024)S(1)} %pad_clamp_fusion.1), kind=kCustom, calls=%fused_computation | custom fusion | bytes 4196352 | tf_op jit(solution)/shard_map/gather | solution.py:142
  141.9 52.0 %all_to_all.10 = bf16[32,1,16,2048]{3,2,1,0:T(8,128)(2,1)S(1)} all-to-all(bf16[32,1,16,2048]{3,2,1,0:T(8,128)(2,1)} %bitcast.188), channel_id=1, replica_groups=mesh['sp'=8,'dp'=4] {'sp','dp'}, dimensions={0} | all-to-all | bytes 4194304 | tf_op jit(solution)/shard_map/all_to_all | solution.py:145
  193.9 1.3 copy-done.5
  195.2 2.2 fusion.37
  197.4 6.3 %fusion.26 = bf16[32,1,16,2048]{3,2,1,0:T(8,128)(2,1)} fusion(bf16[1,512,2048]{2,1,0:T(8,128)(2,1)S(1)} %copy-done, bf16[1,2048,512]{2,1,0:T(8,128)(2,1)} %param.30, bf16[32,1,16,2048]{3,2,1,0:T(8,128)(2,1)} %copy-done.5, f32[32,1,16,512]{3,2,0,1:T(8,128)} %fusion.37), kind=kOutput, calls=%fused_computation.27 | convolution fusion | flops 2150105088 | bytes 9437184 | tf_op jit(solution)/shard_map/nesf,efd->nesd/dot_general | solution.py:80
  203.7 3.8 %all-to-all-start.1 = ((bf16[32,1,16,2048]{3,2,1,0:T(8,128)(2,1)}), bf16[32,1,16,2048]{3,2,1,0:T(8,128)(2,1)}, u32[]{:S(2)}, u32[]{:S(2)}) async-start(bf16[32,1,16,2048]{3,2,1,0:T(8,128)(2,1)} %fusion.26), calls=%async_computation.1 | async-start | bytes 4194304 | tf_op jit(solution)/shard_map/all_to_all | solution.py:150
  207.6 48.5 %all-to-all-done.1 = bf16[32,1,16,2048]{3,2,1,0:T(8,128)(2,1)} async-done(((bf16[32,1,16,2048]{3,2,1,0:T(8,128)(2,1)}), bf16[32,1,16,2048]{3,2,1,0:T(8,128)(2,1)}, u32[]{:S(2)}, u32[]{:S(2)}) %all-to-all-start.1) | async-done | bytes 2097184 | tf_op jit(solution)/shard_map/all_to_all | solution.py:150
  256.2 5.2 %gather_fusion.1 = bf16[256,2048]{1,0:T(8,128)(2,1)} fusion(bf16[512,2048]{1,0:T(8,128)(2,1)} %bitcast.49, s32[1024]{0:T(1024)S(1)} %pad_clamp_fusion), kind=kCustom, calls=%fused_computation.1 | custom fusion | bytes 2098176 | tf_op jit(solution)/shard_map/gather | solution.py:152
  261.4 3.4 %reshape.490 = f32[128,2,2048]{2,1,0:T(2,128)} reshape(bf16[256,2048]{1,0:T(8,128)(2,1)} %gather_fusion.1) | data formatting | bytes 3145728 | tf_op jit(solution)/shard_map/convert_element_type | solution.py:153
  264.7 4.8 %multiply_reduce_fusion = f32[128,2048]{1,0:T(8,128)S(1)} fusion(f32[128,2,2048]{2,1,0:T(2,128)} %reshape.490, f32[128,2]{1,0:T(8,128)S(1)} %copy.38), kind=kLoop, calls=%fused_computation.41 | loop fusion | flops 786432 | bytes 3146752 | tf_op jit(solution)/shard_map/reduce_sum | solution.py:158
  (93 shorter events, 20.4 us)
Async XLA Ops:
  6.5 190.9 %copy-start = (bf16[1,512,2048]{2,1,0:T(8,128)(2,1)S(1)}, bf16[1,512,2048]{2,1,0:T(8,128)(2,1)}, u32[]{:S(2)}) copy-start(bf16[1,512,2048]{2,1,0:T(8,128)(2,1)} %param.31) | copy-start | bytes 6291460
  6.5 45.0 %all-gather.5.cloned.1.call-start = ((), (), s32[]{:S(2)}) async-start(), calls=%async_computation.3 | async-start | bytes 1179648 | tf_op jit(solution)/shard_map/all_gather | solution.py:107
  8.4 84.6 %all-gather.3.cloned.1.call-start = ((), (), s32[]{:S(2)}) async-start(), calls=%async_computation.2 | async-start | bytes 1179648 | tf_op jit(solution)/shard_map/all_gather | solution.py:108
  9.1 4.3 %copy-start.9 = (s32[1,128,2]{1,2,0:T(2,128)S(1)}, s32[1,128,2]{1,2,0:T(2,128)}, u32[]{:S(2)}) copy-start(s32[1,128,2]{1,2,0:T(2,128)} %param.26) | copy-start | bytes 3076
  9.2 4.7 %copy-start.11 = (f32[128]{0:T(128)S(1)}, f32[128]{0:T(128)}, u32[]{:S(2)}) copy-start(f32[128]{0:T(128)} %param.22) | copy-start | bytes 1540
  10.5 0.8 copy-start.2
  11.3 4.0 %copy-start.10 = (f32[128]{0:T(128)S(1)}, f32[128]{0:T(128)}, u32[]{:S(2)}) copy-start(f32[128]{0:T(128)} %param.21) | copy-start | bytes 1540
  54.0 1.0 copy-start.3
  54.0 1.2 copy-start.4
  98.9 1.4 copy-start.1
  108.2 1.4 copy-start.1
  117.6 1.4 copy-start.1
  126.9 1.4 copy-start.1
  132.6 5.0 %copy-start.6 = (bf16[1,128,2048]{2,1,0:T(8,128)(2,1)S(1)}, bf16[1,128,2048]{2,1,0:T(8,128)(2,1)}, u32[]{:S(2)}) copy-start(bf16[1,128,2048]{2,1,0:T(8,128)(2,1)} %param.17) | copy-start | bytes 1572868
  132.6 5.0 %copy-start.7 = (f32[2048]{0:T(1024)S(1)}, f32[2048]{0:T(1024)}, u32[]{:S(2)}) copy-start(f32[2048]{0:T(1024)} %param.24) | copy-start | bytes 24580
  137.6 0.7 copy-start.8
  141.9 53.3 %copy-start.14 = (bf16[1,2048,512]{2,1,0:T(8,128)(2,1)S(1)}, bf16[1,2048,512]{2,1,0:T(8,128)(2,1)}, u32[]{:S(2)}) copy-start(bf16[1,2048,512]{2,1,0:T(8,128)(2,1)} %param.29) | copy-start | bytes 6291460
  193.9 1.3 copy-start.5
  203.7 3.8 %copy-start.12 = (f32[1,128]{1,0:T(1,128)S(1)}, f32[1,128]{1,0:T(1,128)}, u32[]{:S(2)}) copy-start(f32[1,128]{1,0:T(1,128)} %param.28) | copy-start | bytes 1540
  203.7 3.8 %copy-start.13 = (f32[1,128]{1,0:T(1,128)S(1)}, f32[1,128]{1,0:T(1,128)}, u32[]{:S(2)}) copy-start(f32[1,128]{1,0:T(1,128)} %param.27) | copy-start | bytes 1540
  203.7 52.5 %all-to-all-start.1 = ((bf16[32,1,16,2048]{3,2,1,0:T(8,128)(2,1)}), bf16[32,1,16,2048]{3,2,1,0:T(8,128)(2,1)}, u32[]{:S(2)}, u32[]{:S(2)}) async-start(bf16[32,1,16,2048]{3,2,1,0:T(8,128)(2,1)} %fusion.26), calls=%async_computation.1 | async-start | bytes 4194304 | tf_op jit(solution)/shard_map/all_to_all | solution.py:150
Sparse Core Ops, SparseCore 0:
  9.4 42.1 all-gather.4
  53.6 39.2 all-gather.2
where the time goes:
time: 278 us; the launch traced here: 277 us
  waiting for transfers between devices  113 us (41%)
  blocking collectives  52 us (19%)
  matrix products  33.8 us (12%)
  local copies, waits for them, and re-layouts  31 us (11%)
  other arithmetic  23.1 us (8%)
  between operations  13.7 us (5%)
  loops' own time  6.83 us (2%)
  starting transfers between devices  3.84 us (1%)
    all_to_all x1, blocking collectives, local(): lax.all_to_all(shaped, ('sp', 'dp'), split_axis=0, concat_axis=0, tiled=T...  52 us
    all_to_all x1, waiting for transfers between devices, local(): lax.all_to_all(answered, ('sp', 'dp'), split_axis=0, concat_axis=0, tiled...  48.5 us
    all_gather x1, waiting for transfers between devices, local(): lax.all_gather(value_proj, 'sp', axis=1, tiled=True)  37.1 us
    all_gather x1, waiting for transfers between devices, local(): lax.all_gather(key_proj, 'sp', axis=1, tiled=True)  26.7 us
    dot_general x4, matrix products, one_item(): jnp.einsum('gqs,sd->qgd', weights, value_block, preferred_element_type=jn...  14.9 us
    another operation x1, loops' own time, attend_blocks(): results = lax.map(one_item, jnp.arange(blocks * kv_count, dtype=jnp.int32))  6.83 us
    unnamed x31, local copies, waits for them, and re-layouts  6.58 us
    dot_general x1, matrix products, expert_ffn(): jnp.einsum('nesf,efd->nesd', hidden, down_weight, preferred_element_type=...  6.27 us
  transfers between devices with their start and end apart: 3, of which 3 were waited for; matrix products, arithmetic and copies ran while one was open for 7% of the time, Pallas kernels for 0%

commit v1 on v0

v1 whole, which is shorter than its diff:
```python
import functools

import jax
import jax.numpy as jnp
import numpy as np
from jax import lax
from jax.experimental import pallas as pl
from jax.experimental.pallas import tpu as pltpu
from jax.sharding import PartitionSpec as P

HEAD_DIM = 128
GRID_W = 64
GROUPS = 4
EPSILON = 1e-06
MESH = pl.DeviceIdType.MESH
VMEM_LIMIT = 60 * 1024 * 1024
F32 = jnp.float32
BF16 = jnp.bfloat16


def angle_tables(length):
    quarter = HEAD_DIM // 4
    inverse = 10000.0 ** (-np.arange(quarter, dtype=np.float64) / quarter)
    positions = np.arange(length)
    rows = (positions // GRID_W)[:, None] * inverse
    cols = (positions % GRID_W)[:, None] * inverse
    angles = np.concatenate([rows, rows, cols, cols], axis=-1)
    sign = np.where(np.arange(HEAD_DIM) % (2 * quarter) < quarter, -1.0, 1.0)
    return np.cos(angles).astype(np.float32), (np.sin(angles) * sign).astype(np.float32)


def rotate(raw, gain, cos, sin):
    floats = raw.astype(F32)
    normed = floats * lax.rsqrt(jnp.mean(floats * floats, axis=-1, keepdims=True) + EPSILON) * gain
    quarter = HEAD_DIM // 4
    lane = lax.broadcasted_iota(jnp.int32, normed.shape, 1)
    turned = jnp.where(
        (lane & (2 * quarter - 1)) < quarter,
        pltpu.roll(normed, HEAD_DIM - quarter, 1),
        pltpu.roll(normed, quarter, 1),
    )
    return (normed * cos + turned * sin).astype(BF16)


def remote(src, dst, send_sem, recv_sem, device):
    return pltpu.make_async_remote_copy(
        src_ref=src,
        dst_ref=dst,
        send_sem=send_sem,
        recv_sem=recv_sem,
        device_id=device,
        device_id_type=MESH,
    )


def attention_kernel(
    nz, nx,
    q_ref, k_ref, v_ref, qg_ref, kg_ref, cos_ref, sin_ref, res_ref, post_ref, pre_ref, ow_hbm,
    stream_ref, normed_ref,
    k_all, v_all, q_rot, k_rot, att, mixed, ow, ow_sem,
    rk, rv, skx, sku, skd, svx, svu, svd,
):
    tokens, width = q_ref.shape
    heads = width // HEAD_DIM
    kv_heads = k_ref.shape[1] // HEAD_DIM
    group = heads // kv_heads
    me = lax.axis_index("sp")
    dp = lax.axis_index("dp")
    z, x = me // nx, me % nx
    up, down = (me + nx, dp), (me - nx, dp)
    has_up, has_down = z < nz - 1, z > 0

    load_ow = pltpu.make_async_copy(ow_hbm, ow, ow_sem)
    load_ow.start()

    barrier = pltpu.get_barrier_semaphore()
    around = [(lax.rem(z + 1, nz) * nx + x, dp), (lax.rem(z + nz - 1, nz) * nx + x, dp)]
    beside = [(z * nx + lax.rem(x + off, nx), dp) for off in range(1, nx)]
    for device in around + beside:
        pl.semaphore_signal(barrier, inc=1, device_id=device, device_id_type=MESH)
    pl.semaphore_wait(barrier, len(around) + len(beside))

    def pass_on(src, buf, recv, send_up, send_down, slot, when_up, when_down):
        @pl.when(when_up)
        def _():
            remote(src, buf.at[slot], send_up.at[slot], recv.at[slot], up).start()

        @pl.when(when_down)
        def _():
            remote(src, buf.at[slot], send_down.at[slot], recv.at[slot], down).start()

    def spread(src, slot):
        for off in range(1, nx):
            remote(
                src, v_all.at[slot], svx.at[slot, off], rv.at[slot], beside[off - 1]
            ).start()

    for off in range(1, nx):
        remote(k_ref, k_all.at[me], skx.at[off], rk.at[me], beside[off - 1]).start()
    pass_on(k_ref, k_all, rk, sku, skd, me, has_up, has_down)
    pass_on(v_ref, v_all, rv, svu, svd, me, has_up, has_down)
    spread(v_ref, me)

    def arrived(buf, recv, slot):
        remote(buf.at[slot], buf.at[slot], recv.at[slot], recv.at[slot], up).wait_recv()

    def place_keys(src, slot):
        start = pl.multiple_of(slot * tokens, tokens)
        cos = cos_ref[pl.ds(start, tokens), :]
        sin = sin_ref[pl.ds(start, tokens), :]
        for head in range(kv_heads):
            k_rot[head, pl.ds(start, tokens), :] = rotate(
                src[:, head * HEAD_DIM : (head + 1) * HEAD_DIM], kg_ref[...], cos, sin
            )

    own = pl.multiple_of(me * tokens, tokens)
    q_cos = cos_ref[pl.ds(own, tokens), :]
    q_sin = sin_ref[pl.ds(own, tokens), :]
    for head in range(heads):
        q_rot[head] = rotate(
            q_ref[:, head * HEAD_DIM : (head + 1) * HEAD_DIM], qg_ref[...], q_cos, q_sin
        )
    v_all[me] = v_ref[...]

    for off in range(1, nx):
        slot = z * nx + lax.rem(x + off, nx)
        arrived(k_all, rk, slot)
        pass_on(k_all.at[slot], k_all, rk, sku, skd, slot, has_up, has_down)
    place_keys(k_ref, me)
    for off in range(1, nx):
        slot = z * nx + lax.rem(x + off, nx)
        place_keys(k_all.at[slot], slot)

    for dist in range(1, nz):
        for below in (True, False):
            source = z - dist if below else z + dist
            present = source >= 0 if below else source < nz

            @pl.when(present)
            def _(source=source, below=below):
                for off in range(nx):
                    slot = source * nx + lax.rem(x + off, nx)
                    arrived(k_all, rk, slot)
                    pass_on(
                        k_all.at[slot], k_all, rk, sku, skd, slot,
                        has_up if below else False, False if below else has_down,
                    )
                slot = source * nx + x
                arrived(v_all, rv, slot)
                pass_on(
                    v_all.at[slot], v_all, rv, svu, svd, slot,
                    has_up if below else False, False if below else has_down,
                )
                spread(v_all.at[slot], slot)
                for off in range(nx):
                    slot = source * nx + lax.rem(x + off, nx)
                    place_keys(k_all.at[slot], slot)

    for plane in range(nz):
        for off in range(1, nx):
            arrived(v_all, rv, plane * nx + lax.rem(x + off, nx))

    length = nz * nx * tokens
    factor = float(HEAD_DIM**-0.5 * np.log2(np.e))

    def one_group(kv, carry):
        lanes = pl.ds(pl.multiple_of(kv * HEAD_DIM, HEAD_DIM), HEAD_DIM)
        keys = k_rot[kv]
        values = v_all[:, :, lanes].reshape(length, HEAD_DIM)
        for member in range(group):
            head = kv * group + member
            scores = lax.dot_general(
                q_rot[head], keys, (((1,), (1,)), ((), ())), preferred_element_type=F32
            )
            top = jnp.max(scores, axis=-1, keepdims=True)
            raised = jnp.exp2((scores - top) * factor)
            probs = (raised * (1.0 / jnp.sum(raised, axis=-1, keepdims=True))).astype(BF16)
            columns = pl.ds(pl.multiple_of(head * HEAD_DIM, HEAD_DIM), HEAD_DIM)
            att[:, columns] = jnp.dot(probs, values, preferred_element_type=F32).astype(BF16)
        return carry

    lax.fori_loop(0, kv_heads, one_group, 0)

    load_ow.wait()
    tile = 512

    def one_tile(step, carry):
        columns = pl.ds(pl.multiple_of(step * tile, tile), tile)
        mixed[:, columns] = jnp.dot(
            att[...], ow[:, columns], preferred_element_type=F32
        ).astype(BF16)
        return carry

    lax.fori_loop(0, width // tile, one_tile, 0)

    blend = mixed[...].astype(F32)
    blend = blend * lax.rsqrt(jnp.mean(blend * blend, axis=-1, keepdims=True) + EPSILON)
    stream = (res_ref[...].astype(F32) + blend * post_ref[...]).astype(BF16)
    stream_ref[...] = stream
    wide = stream.astype(F32)
    wide = wide * lax.rsqrt(jnp.mean(wide * wide, axis=-1, keepdims=True) + EPSILON)
    normed_ref[...] = (wide * pre_ref[...]).astype(BF16)

    def sent(src, sem, device):
        remote(src, src, sem, sem, device).wait_send()

    for off in range(1, nx):
        sent(k_ref, skx.at[off], beside[off - 1])
    for plane in range(nz):
        for off in range(nx):
            slot = plane * nx + lax.rem(x + off, nx)

            @pl.when(jnp.logical_and(has_up, z >= plane))
            def _(slot=slot, off=off):
                sent(k_all.at[slot], sku.at[slot], up)
                if off == 0:
                    sent(v_all.at[slot], svu.at[slot], up)

            @pl.when(jnp.logical_and(has_down, z <= plane))
            def _(slot=slot, off=off):
                sent(k_all.at[slot], skd.at[slot], down)
                if off == 0:
                    sent(v_all.at[slot], svd.at[slot], down)

        slot = plane * nx + x
        for off in range(1, nx):
            sent(v_all.at[slot], svx.at[slot, off], beside[off - 1])


def before(tokens):
    row = lax.broadcasted_iota(jnp.int32, (tokens, tokens), 0)
    col = lax.broadcasted_iota(jnp.int32, (tokens, tokens), 1)
    return (row < col).astype(F32).astype(BF16)


def group_choice(meta, first_expert, count, rows):
    tokens = meta.shape[1]
    low = first_expert.astype(F32)
    member = jnp.where((meta[0:1] >= low) & (meta[0:1] < low + float(count)), 1.0, 0.0)
    rank = jnp.dot(
        jnp.broadcast_to(member, (8, tokens)).astype(BF16),
        before(tokens),
        preferred_element_type=F32,
    )[0:1]
    place = lax.broadcasted_iota(jnp.int32, (rows, tokens), 0).astype(F32)
    return jnp.where(rank == place, 1.0, 0.0) * member


def slot_choice(meta, first_expert, count, cap):
    tokens = meta.shape[1]
    names = lax.broadcasted_iota(jnp.int32, (count, tokens), 0).astype(F32)
    names = names + first_expert.astype(F32)
    first = jnp.where(meta[0:1] == names, 1.0, 0.0)
    second = jnp.where(meta[1:2] == names, 1.0, 0.0)
    rank = jnp.dot((first + second).astype(BF16), before(tokens), preferred_element_type=F32)
    row = lax.broadcasted_iota(jnp.int32, (count * cap, count), 0)
    start = lax.broadcasted_iota(jnp.int32, (count * cap, count), 1) * cap
    widen = jnp.where((row >= start) & (row < start + cap), 1.0, 0.0).astype(BF16)

    def widened(values):
        return jnp.dot(widen, values.astype(BF16), preferred_element_type=F32)

    place = lax.broadcasted_iota(jnp.int32, (count * cap, tokens), 0) & (cap - 1)
    hit = jnp.where(widened(rank) == place.astype(F32), 1.0, 0.0)
    return widened(first) * hit, widened(second) * hit


def contract(left, right, dims):
    return lax.dot_general(
        left.astype(BF16), right.astype(BF16), ((dims[:1], dims[1:]), ((), ())),
        preferred_element_type=F32,
    )


def expert_kernel(
    nz, nx, n_dp,
    normed_ref, stream_ref, meta_ref, wg_hbm, wu_hbm, wd_hbm,
    out_ref,
    wg, wu, wd, w_sem, p1, r1, metas, p2, r2, o2, back, mix, fin,
    s1, t1, sm, tm, s2, t2, s3, t3, s4, t4,
):
    tokens, width = normed_ref.shape
    count, cap = p2.shape[1], p2.shape[2]
    rows = p1.shape[1]
    sp = lax.axis_index("sp")
    dp = lax.axis_index("dp")
    z, x = sp // nx, sp % nx
    me = x * n_dp + dp

    loads = [
        pltpu.make_async_copy(src, dst, w_sem.at[i])
        for i, (src, dst) in enumerate(((wg_hbm, wg), (wu_hbm, wu), (wd_hbm, wd)))
    ]
    for load in loads:
        load.start()

    def plane_peer(off):
        j = lax.rem(me + off, count)
        return j, (z * nx + j // n_dp, j % n_dp)

    def column_peer(dist):
        plane = lax.rem(z + dist, nz)
        return plane, (plane * nx + x, dp)

    barrier = pltpu.get_barrier_semaphore()
    for off in range(1, count):
        pl.semaphore_signal(barrier, inc=1, device_id=plane_peer(off)[1], device_id_type=MESH)
    for dist in range(1, nz):
        pl.semaphore_signal(barrier, inc=1, device_id=column_peer(dist)[1], device_id_type=MESH)

    meta = meta_ref[...]
    for g in range(nz):
        pick = group_choice(meta, jnp.int32(g * count), count, rows)
        p1[g] = contract(pick, normed_ref[...], (1, 0)).astype(BF16)
    metas[z] = meta
    r1[z] = p1[z]

    pl.semaphore_wait(barrier, count - 1 + nz - 1)
    for dist in range(1, nz):
        plane, device = column_peer(dist)
        remote(meta_ref, metas.at[z], sm.at[plane], tm.at[z], device).start()
        remote(p1.at[plane], r1.at[z], s1.at[plane], t1.at[z], device).start()

    first_expert = z * count

    def dispatch(dist, carry):
        source, device = column_peer(dist)

        @pl.when(dist > 0)
        def _():
            remote(meta_ref, metas.at[source], sm.at[source], tm.at[source], device).wait_recv()
            remote(p1.at[source], r1.at[source], s1.at[source], t1.at[source], device).wait_recv()

        got = metas[source]
        group = group_choice(got, first_expert, count, rows)
        first, second = slot_choice(got, first_expert, count, cap)
        pick = contract(first + second, group, (1, 1))
        packed = contract(pick, r1[source], (1, 0)).astype(BF16)
        p2[source] = packed.reshape(count, cap, width)
        r2[source, me] = p2[source, me]
        for off in range(1, count):
            j, device = plane_peer(off)
            remote(
                p2.at[source, j], r2.at[source, me], s2.at[source, j], t2.at[source, me], device
            ).start()
        return carry

    lax.fori_loop(0, nz, dispatch, 0)
    for load in loads:
        load.wait()

    def transform(dist, carry):
        source = lax.rem(z + dist, nz)
        for off in range(1, count):
            j, device = plane_peer(off)
            remote(
                p2.at[source, j], r2.at[source, j], s2.at[source, j], t2.at[source, j], device
            ).wait_recv()
        arrived = r2[source].reshape(count * cap, width)
        gated = jnp.dot(arrived, wg[...], preferred_element_type=F32)
        lifted = jnp.dot(arrived, wu[...], preferred_element_type=F32)
        hidden = (gated / (1.0 + jnp.exp(-gated)) * lifted).astype(BF16)
        result = jnp.dot(hidden, wd[...], preferred_element_type=F32).astype(BF16)
        o2[source] = result.reshape(count, cap, width)
        back[source, me] = o2[source, me]
        for off in range(1, count):
            j, device = plane_peer(off)
            remote(
                o2.at[source, j], back.at[source, me], s3.at[source, j], t3.at[source, me], device
            ).start()
        return carry

    lax.fori_loop(0, nz, transform, 0)

    def combine(dist, carry):
        source, column = column_peer(dist)
        for off in range(1, count):
            j, device = plane_peer(off)
            remote(
                o2.at[source, j], back.at[source, j], s3.at[source, j], t3.at[source, j], device
            ).wait_recv()
        got = metas[source]
        group = group_choice(got, first_expert, count, rows)
        first, second = slot_choice(got, first_expert, count, cap)
        outs = back[source].reshape(count * cap, width)
        one = contract(contract(group, first, (1, 1)), outs, (1, 0))
        two = contract(contract(group, second, (1, 1)), outs, (1, 0))
        weight = jnp.sum(group * got[2:3], axis=1, keepdims=True)
        share = jnp.sum(group * got[3:4], axis=1, keepdims=True)
        total = (weight * (share * one + (1.0 - share) * two)).astype(BF16)
        mix[source] = total

        @pl.when(dist == 0)
        def _():
            fin[source] = total

        @pl.when(dist > 0)
        def _():
            remote(mix.at[source], fin.at[z], s4.at[source], t4.at[z], column).start()

        return carry

    lax.fori_loop(0, nz, combine, 0)

    picks = [
        group_choice(meta, jnp.int32(g * count), count, rows) for g in range(nz)
    ]
    for dist in range(1, nz):
        plane, device = column_peer(dist)
        remote(mix.at[plane], fin.at[plane], s4.at[plane], t4.at[plane], device).wait_recv()
    every = jnp.concatenate(picks, axis=0)
    added = contract(every, fin[...].reshape(tokens, width), (0, 0))
    out_ref[...] = (stream_ref[...].astype(F32) + added).astype(BF16)

    for dist in range(1, nz):
        plane, device = column_peer(dist)
        remote(meta_ref, metas.at[z], sm.at[plane], tm.at[z], device).wait_send()
        remote(p1.at[plane], r1.at[z], s1.at[plane], t1.at[z], device).wait_send()
        remote(mix.at[plane], fin.at[z], s4.at[plane], t4.at[z], device).wait_send()

    def drain(source, carry):
        for off in range(1, count):
            j, device = plane_peer(off)
            remote(
                p2.at[source, j], r2.at[source, me], s2.at[source, j], t2.at[source, me], device
            ).wait_send()
            remote(
                o2.at[source, j], back.at[source, me], s3.at[source, j], t3.at[source, me], device
            ).wait_send()
        return carry

    lax.fori_loop(0, nz, drain, 0)


def local(
    residual_in, query_proj, key_proj, value_proj, query_gain, key_gain, out_weight, post_gain,
    pre_gain, route_ids, group_weight, first_share, gate_weight, up_weight, down_weight,
):
    n_sp = lax.axis_size("sp")
    n_dp = lax.axis_size("dp")
    tokens, width = query_proj.shape[1:]
    kv_width = key_proj.shape[2]
    heads, kv_heads = width // HEAD_DIM, kv_width // HEAD_DIM
    nz = GROUPS
    nx = n_sp // nz
    length = n_sp * tokens
    cos, sin = angle_tables(length)
    vmem = pl.BlockSpec(memory_space=pltpu.VMEM)
    hbm = pl.BlockSpec(memory_space=pl.ANY)
    dma = pltpu.SemaphoreType.DMA
    row = jax.ShapeDtypeStruct((tokens, width), BF16)
    stream, normed = pl.pallas_call(
        functools.partial(attention_kernel, nz, nx),
        out_shape=(row, row),
        in_specs=[vmem] * 10 + [hbm],
        out_specs=(vmem, vmem),
        scratch_shapes=[
            pltpu.VMEM((n_sp, tokens, kv_width), BF16),
            pltpu.VMEM((n_sp, tokens, kv_width), BF16),
            pltpu.VMEM((heads, tokens, HEAD_DIM), BF16),
            pltpu.VMEM((kv_heads, length, HEAD_DIM), BF16),
            pltpu.VMEM((tokens, width), BF16),
            pltpu.VMEM((tokens, width), BF16),
            pltpu.VMEM((width, width), BF16),
            dma,
            dma((n_sp,)), dma((n_sp,)),
            dma((nx,)), dma((n_sp,)), dma((n_sp,)),
            dma((n_sp, nx)), dma((n_sp,)), dma((n_sp,)),
        ],
        compiler_params=pltpu.CompilerParams(
            collective_id=0, has_side_effects=True, vmem_limit_bytes=VMEM_LIMIT
        ),
        name="attention",
    )(
        query_proj[0], key_proj[0], value_proj[0],
        query_gain.reshape(1, -1), key_gain.reshape(1, -1),
        jnp.asarray(cos), jnp.asarray(sin),
        residual_in[0], post_gain.reshape(1, -1), pre_gain.reshape(1, -1), out_weight,
    )

    experts = gate_weight.shape[0] * n_sp * n_dp
    count = experts // nz
    cap = max(16, 4 * tokens // experts)
    rows = tokens // nz
    ff = gate_weight.shape[2]
    meta = jnp.concatenate(
        [route_ids[0].T.astype(F32), group_weight, first_share, jnp.zeros((4, tokens), F32)], axis=0
    )
    blocks = pltpu.VMEM((nz, count, cap, width), BF16)
    lines = pltpu.VMEM((nz, rows, width), BF16)
    out = pl.pallas_call(
        functools.partial(expert_kernel, nz, nx, n_dp),
        out_shape=row,
        in_specs=[vmem] * 3 + [hbm] * 3,
        out_specs=vmem,
        scratch_shapes=[
            pltpu.VMEM((width, ff), BF16),
            pltpu.VMEM((width, ff), BF16),
            pltpu.VMEM((ff, width), BF16),
            dma((3,)),
            lines, lines,
            pltpu.VMEM((nz, 8, tokens), F32),
            blocks, blocks, blocks, blocks,
            lines, lines,
            dma((nz,)), dma((nz,)), dma((nz,)), dma((nz,)),
            dma((nz, count)), dma((nz, count)), dma((nz, count)), dma((nz, count)),
            dma((nz,)), dma((nz,)),
        ],
        compiler_params=pltpu.CompilerParams(
            collective_id=1, has_side_effects=True, vmem_limit_bytes=VMEM_LIMIT
        ),
        name="experts",
    )(normed, stream, meta, gate_weight[0], up_weight[0], down_weight[0])
    return out.reshape(1, tokens, width)


def solution(mesh):
    tok3 = P("dp", "sp", None)
    tok2 = P("dp", "sp")
    weight = P(("sp", "dp"), None, None)
    placed = (
        tok3, tok3, tok3, tok3, P(), P(), P(), P(), P(), tok3, tok2, tok2, weight, weight, weight,
    )
    return jax.shard_map(
        local, mesh=mesh, in_specs=placed, out_specs=P("dp", "sp", None), check_vma=False
    )
```

time: 278 us -> 118 us (0.42)
  Pallas kernels: 0 us -> 114 us
  waiting for transfers between devices: 113 us -> 0 us
  blocking collectives: 52 us -> 0 us
  matrix products: 33.8 us -> 0 us
  local copies, waits for them, and re-layouts: 31 us -> 1.96 us
  other arithmetic: 23.1 us -> 2.01 us
  between operations: 13.7 us -> 0.02 us
  loops' own time: 6.83 us -> 0 us
  starting transfers between devices: 3.84 us -> 0 us
    pallas_call x0 -> x2, Pallas kernels: none -> 114 us  [the longest x1 62.1 us: local(): pl.pallas_call(functools.partial(expert_kernel, nz, nx, n_dp), out_shape=...]
    all_gather x2 -> x0, waiting for transfers between devices: 63.8 us -> none  [the longest x1 37.1 us: local(): lax.all_gather(value_proj, 'sp', axis=1, tiled=True)]
    all_to_all x1 -> x0, blocking collectives: 52 us -> none  [local(): lax.all_to_all(shaped, ('sp', 'dp'), split_axis=0, concat_axis=0, tiled=T...]
    all_to_all x1 -> x0, waiting for transfers between devices: 48.5 us -> none  [local(): lax.all_to_all(answered, ('sp', 'dp'), split_axis=0, concat_axis=0, tiled...]
    dot_general x11 -> x0, matrix products: 33.8 us -> none  [the longest x4 14.9 us: one_item(): jnp.einsum('gqs,sd->qgd', weights, value_block, preferred_element_type=jn...]
    gather x2 -> x0, local copies, waits for them, and re-layouts: 8.55 us -> none  [the longest x1 5.2 us: local(): returned.reshape(expert_count * capacity, model_width)[slot_index]]
    another operation x1 -> x0, loops' own time: 6.83 us -> none  [attend_blocks(): results = lax.map(one_item, jnp.arange(blocks * kv_count, dtype=jnp.int32))]
    reduce_sum x5 -> x0, other arithmetic: 6.81 us -> none  [the longest x1 4.81 us: local(): combined = jnp.sum(weight_pair[:, :, None] * results, axis=1)]
  transfers between devices with their start and end apart: 3 -> 0, of which waited for: 3 -> 0; matrix products, arithmetic and copies ran while one was open for 7% -> 0% of each run, Pallas kernels for 0% -> 0%
where the time goes in v1:
time: 118 us
  Pallas kernels  114 us (97%)
  other arithmetic  2.01 us (2%)
  local copies, waits for them, and re-layouts  1.96 us (2%)
    pallas_call x1, Pallas kernels, local(): pl.pallas_call(functools.partial(expert_kernel, nz, nx, n_dp), out_shape=...  62.1 us
    pallas_call x1, Pallas kernels, local(): pl.pallas_call(functools.partial(attention_kernel, nz, nx), out_shape=(ro...  51.5 us

profile of v1, /device:TPU:0, one launch (start us, length us, event | category | flops | bytes accessed | tf_op | source)
XLA Modules:
  0.0 117.5 jit_solution(9712836727385682449)
XLA Ops:
  0.0 0.1 pad.3.clone
  0.1 0.7 convert_bitcast_fusion
  0.8 1.3 %maximum_maximum_fusion.meta_ref = f32[8,128]{1,0:T(8,128)} fusion(f32[1,128]{1,0:T(1,128)} %param.28, f32[1,128]{1,0:T(1,128)} %param.27, f32[2,128]{1,0:T(2,128)S(1)} %convert_bitcast_fusion, f32[8]{0:T(128)S(1)} %pad.3.clone), kind=kLoop, calls=%fused_computation | loop fusion | flops 3072 | bytes 6176 | tf_op jit(solution)/shard_map/concatenate | solution.py:486
  2.1 51.5 %attention.1 = (bf16[128,2048]{1,0:T(8,128)(2,1)}, bf16[128,2048]{1,0:T(8,128)(2,1)}) custom-call(bf16[128,2048]{1,0:T(8,128)(2,1)} %bitcast.20, bf16[128,512]{1,0:T(8,128)(2,1)} %bitcast.22, bf16[128,512]{1,0:T(8,128)(2,1)} %bitcast.23, f32[1,128]{1,0:T(1,128)} %bitcast.26, f32[1,128]{1,0:T(1,128)} %bitcast.27, f32[1024,128]{1,0:T(8,128)} %constant.6.clone.cos_ref, ...), custom_call_target="tpu_custom_call" | custom-call | tf_op jit(solution)/shard_map/attention/pallas_call | solution.py:452
  53.6 62.1 %experts.1 = bf16[128,2048]{1,0:T(8,128)(2,1)} custom-call(bf16[128,2048]{1,0:T(8,128)(2,1)} %get-tuple-element.7.normed_ref, bf16[128,2048]{1,0:T(8,128)(2,1)} %get-tuple-element.8.stream_ref, f32[8,128]{1,0:T(8,128)} %maximum_maximum_fusion.meta_ref, bf16[2048,512]{1,0:T(8,128)(2,1)} %bitcast.16, bf16[2048,512]{1,0:T(8,128)(2,1)} %bitcast.17, ...), custom_call_target="tpu_custom_call" | custom-call | tf_op jit(solution)/shard_map/experts/pallas_call | solution.py:491
  115.7 1.9 %copy.19 = bf16[1,128,2048]{2,1,0:T(8,128)(2,1)} copy(bf16[1,128,2048]{2,1,0:T(8,128)(2,1)} %bitcast.19) | data formatting | bytes 1048576
  (1 shorter events, 0.0 us)

commit v2 on v1

--- a/solution.py
+++ b/solution.py
@@ -57,7 +57,7 @@
     nz, nx,
     q_ref, k_ref, v_ref, qg_ref, kg_ref, cos_ref, sin_ref, res_ref, post_ref, pre_ref, ow_hbm,
     stream_ref, normed_ref,
-    k_all, v_all, q_rot, k_rot, att, mixed, ow, ow_sem,
+    k_all, v_all, q_rot, k_rot, att, acc, ow, ow_sem,
     rk, rv, skx, sku, skd, svx, svu, svd,
 ):
     tokens, width = q_ref.shape
@@ -69,6 +69,7 @@
     z, x = me // nx, me % nx
     up, down = (me + nx, dp), (me - nx, dp)
     has_up, has_down = z < nz - 1, z > 0
+    both = ((k_ref, k_all, rk, skx, sku, skd), (v_ref, v_all, rv, svx, svu, svd))
 
     load_ow = pltpu.make_async_copy(ow_hbm, ow, ow_sem)
     load_ow.start()
@@ -80,39 +81,100 @@
         pl.semaphore_signal(barrier, inc=1, device_id=device, device_id_type=MESH)
     pl.semaphore_wait(barrier, len(around) + len(beside))
 
-    def pass_on(src, buf, recv, send_up, send_down, slot, when_up, when_down):
-        @pl.when(when_up)
-        def _():
-            remote(src, buf.at[slot], send_up.at[slot], recv.at[slot], up).start()
-
-        @pl.when(when_down)
-        def _():
-            remote(src, buf.at[slot], send_down.at[slot], recv.at[slot], down).start()
-
-    def spread(src, slot):
-        for off in range(1, nx):
-            remote(
-                src, v_all.at[slot], svx.at[slot, off], rv.at[slot], beside[off - 1]
-            ).start()
-
-    for off in range(1, nx):
-        remote(k_ref, k_all.at[me], skx.at[off], rk.at[me], beside[off - 1]).start()
-    pass_on(k_ref, k_all, rk, sku, skd, me, has_up, has_down)
-    pass_on(v_ref, v_all, rv, svu, svd, me, has_up, has_down)
-    spread(v_ref, me)
-
-    def arrived(buf, recv, slot):
-        remote(buf.at[slot], buf.at[slot], recv.at[slot], recv.at[slot], up).wait_recv()
-
-    def place_keys(src, slot):
-        start = pl.multiple_of(slot * tokens, tokens)
-        cos = cos_ref[pl.ds(start, tokens), :]
-        sin = sin_ref[pl.ds(start, tokens), :]
-        for head in range(kv_heads):
-            k_rot[head, pl.ds(start, tokens), :] = rotate(
-                src[:, head * HEAD_DIM : (head + 1) * HEAD_DIM], kg_ref[...], cos, sin
+    def lanes_of(head):
+        return pl.ds(pl.multiple_of(head * HEAD_DIM, HEAD_DIM), HEAD_DIM)
+
+    def hop(src, buf, recv, send, slot, head, device):
+        return remote(src, buf.at[slot, head], send, recv.at[slot, head], device)
+
+    def send_own(head):
+        for raw, buf, recv, sx, su, sd in both:
+            src = raw.at[:, lanes_of(head)]
+
+            @pl.when(has_up)
+            def _():
+                hop(src, buf, recv, su.at[me, head], me, head, up).start()
+
+            @pl.when(has_down)
+            def _():
+                hop(src, buf, recv, sd.at[me, head], me, head, down).start()
+
+        for raw, buf, recv, sx, su, sd in both:
+            src = raw.at[:, lanes_of(head)]
+            for off in range(1, nx):
+                hop(src, buf, recv, sx.at[me, head, off], me, head, beside[off - 1]).start()
+
+    def arrived(buf, recv, slot, head):
+        block = buf.at[slot, head]
+        remote(block, block, recv.at[slot, head], recv.at[slot, head], up).wait_recv()
+
+    def relay(head):
+        for dist in range(1, nz):
+            for below in (True, False):
+                source = z - dist if below else z + dist
+                present = source >= 0 if below else source < nz
+                further = has_up if below else has_down
+                onward = up if below else down
+
+                @pl.when(present)
+                def _(source=source, below=below, further=further, onward=onward):
+                    slot = source * nx + x
+                    for _raw, buf, recv, sx, su, sd in both:
+                        arrived(buf, recv, slot, head)
+                        src = buf.at[slot, head]
+                        send = su if below else sd
+
+                        @pl.when(further)
+                        def _(src=src, buf=buf, recv=recv, send=send):
+                            hop(src, buf, recv, send.at[slot, head], slot, head, onward).start()
+
+                        for off in range(1, nx):
+                            hop(
+                                src, buf, recv, sx.at[slot, head, off], slot, head,
+                                beside[off - 1],
+                            ).start()
+
+    length = nz * nx * tokens
+    factor = float(HEAD_DIM**-0.5 * np.log2(np.e))
+    span = group * HEAD_DIM
+
+    def attend(kv):
+        for plane in range(nz):
+            for off in range(1, nx):
+                slot = plane * nx + lax.rem(x + off, nx)
+                arrived(k_all, rk, slot, kv)
+                arrived(v_all, rv, slot, kv)
+        k_all[me, kv] = k_ref[:, lanes_of(kv)]
+        v_all[me, kv] = v_ref[:, lanes_of(kv)]
+
+        def place(slot, carry):
+            rows = pl.ds(pl.multiple_of(slot * tokens, tokens), tokens)
+            k_rot[rows, :] = rotate(k_all[slot, kv], kg_ref[...], cos_ref[rows, :], sin_ref[rows, :])
+            return carry
+
+        lax.fori_loop(0, nz * nx, place, 0)
+        keys = k_rot[...]
+        values = v_all[:, kv].reshape(length, HEAD_DIM)
+        for member in range(group):
+            scores = lax.dot_general(
+                q_rot[kv * group + member], keys, (((1,), (1,)), ((), ())),
+                preferred_element_type=F32,
             )
-
+            top = jnp.max(scores, axis=-1, keepdims=True)
+            raised = jnp.exp2((scores - top) * factor)
+            probs = (raised * (1.0 / jnp.sum(raised, axis=-1, keepdims=True))).astype(BF16)
+            att[:, member * HEAD_DIM : (member + 1) * HEAD_DIM] = jnp.dot(
+                probs, values, preferred_element_type=F32
+            ).astype(BF16)
+        part = ow.at[pl.ds(pl.multiple_of(kv * span, span), span), :]
+        tile = 1024
+        for start in range(0, width, tile):
+            columns = slice(start, start + tile)
+            acc[:, columns] += jnp.dot(att[...], part[:, columns], preferred_element_type=F32)
+
+    send_own(0)
+    for head in range(1, min(3, kv_heads)):
+        send_own(head)
     own = pl.multiple_of(me * tokens, tokens)
     q_cos = cos_ref[pl.ds(own, tokens), :]
     q_sin = sin_ref[pl.ds(own, tokens), :]
@@ -120,80 +182,25 @@
         q_rot[head] = rotate(
             q_ref[:, head * HEAD_DIM : (head + 1) * HEAD_DIM], qg_ref[...], q_cos, q_sin
         )
-    v_all[me] = v_ref[...]
-
-    for off in range(1, nx):
-        slot = z * nx + lax.rem(x + off, nx)
-        arrived(k_all, rk, slot)
-        pass_on(k_all.at[slot], k_all, rk, sku, skd, slot, has_up, has_down)
-    place_keys(k_ref, me)
-    for off in range(1, nx):
-        slot = z * nx + lax.rem(x + off, nx)
-        place_keys(k_all.at[slot], slot)
-
-    for dist in range(1, nz):
-        for below in (True, False):
-            source = z - dist if below else z + dist
-            present = source >= 0 if below else source < nz
-
-            @pl.when(present)
-            def _(source=source, below=below):
-                for off in range(nx):
-                    slot = source * nx + lax.rem(x + off, nx)
-                    arrived(k_all, rk, slot)
-                    pass_on(
-                        k_all.at[slot], k_all, rk, sku, skd, slot,
-                        has_up if below else False, False if below else has_down,
-                    )
-                slot = source * nx + x
-                arrived(v_all, rv, slot)
-                pass_on(
-                    v_all.at[slot], v_all, rv, svu, svd, slot,
-                    has_up if below else False, False if below else has_down,
-                )
-                spread(v_all.at[slot], slot)
-                for off in range(nx):
-                    slot = source * nx + lax.rem(x + off, nx)
-                    place_keys(k_all.at[slot], slot)
-
-    for plane in range(nz):
-        for off in range(1, nx):
-            arrived(v_all, rv, plane * nx + lax.rem(x + off, nx))
-
-    length = nz * nx * tokens
-    factor = float(HEAD_DIM**-0.5 * np.log2(np.e))
-
-    def one_group(kv, carry):
-        lanes = pl.ds(pl.multiple_of(kv * HEAD_DIM, HEAD_DIM), HEAD_DIM)
-        keys = k_rot[kv]
-        values = v_all[:, :, lanes].reshape(length, HEAD_DIM)
-        for member in range(group):
-            head = kv * group + member
-            scores = lax.dot_general(
-                q_rot[head], keys, (((1,), (1,)), ((), ())), preferred_element_type=F32
-            )
-            top = jnp.max(scores, axis=-1, keepdims=True)
-            raised = jnp.exp2((scores - top) * factor)
-            probs = (raised * (1.0 / jnp.sum(raised, axis=-1, keepdims=True))).astype(BF16)
-            columns = pl.ds(pl.multiple_of(head * HEAD_DIM, HEAD_DIM), HEAD_DIM)
-            att[:, columns] = jnp.dot(probs, values, preferred_element_type=F32).astype(BF16)
+    acc[...] = jnp.zeros_like(acc)
+    relay(0)
+    load_ow.wait()
+
+    def one_head(kv, carry):
+        @pl.when(kv + 3 < kv_heads)
+        def _():
+            send_own(kv + 3)
+
+        @pl.when(kv + 1 < kv_heads)
+        def _():
+            relay(kv + 1)
+
+        attend(kv)
         return carry
 
-    lax.fori_loop(0, kv_heads, one_group, 0)
-
-    load_ow.wait()
-    tile = 512
-
-    def one_tile(step, carry):
-        columns = pl.ds(pl.multiple_of(step * tile, tile), tile)
-        mixed[:, columns] = jnp.dot(
-            att[...], ow[:, columns], preferred_element_type=F32
-        ).astype(BF16)
-        return carry
-
-    lax.fori_loop(0, width // tile, one_tile, 0)
-
-    blend = mixed[...].astype(F32)
+    lax.fori_loop(0, kv_heads, one_head, 0)
+
+    blend = acc[...].astype(BF16).astype(F32)
     blend = blend * lax.rsqrt(jnp.mean(blend * blend, axis=-1, keepdims=True) + EPSILON)
     stream = (res_ref[...].astype(F32) + blend * post_ref[...]).astype(BF16)
     stream_ref[...] = stream
@@ -201,30 +208,28 @@
     wide = wide * lax.rsqrt(jnp.mean(wide * wide, axis=-1, keepdims=True) + EPSILON)
     normed_ref[...] = (wide * pre_ref[...]).astype(BF16)
 
-    def sent(src, sem, device):
-        remote(src, src, sem, sem, device).wait_send()
-
-    for off in range(1, nx):
-        sent(k_ref, skx.at[off], beside[off - 1])
-    for plane in range(nz):
-        for off in range(nx):
-            slot = plane * nx + lax.rem(x + off, nx)
-
-            @pl.when(jnp.logical_and(has_up, z >= plane))
-            def _(slot=slot, off=off):
-                sent(k_all.at[slot], sku.at[slot], up)
-                if off == 0:
-                    sent(v_all.at[slot], svu.at[slot], up)
-
-            @pl.when(jnp.logical_and(has_down, z <= plane))
-            def _(slot=slot, off=off):
-                sent(k_all.at[slot], skd.at[slot], down)
-                if off == 0:
-                    sent(v_all.at[slot], svd.at[slot], down)
-
-        slot = plane * nx + x
-        for off in range(1, nx):
-            sent(v_all.at[slot], svx.at[slot, off], beside[off - 1])
+    def sent(buf, sem, device):
+        block = buf.at[0, 0]
+        remote(block, block, sem, sem, device).wait_send()
+
+    def drain(head, carry):
+        for _raw, buf, recv, sx, su, sd in both:
+            for plane in range(nz):
+                slot = plane * nx + x
+
+                @pl.when(jnp.logical_and(has_up, z >= plane))
+                def _(slot=slot):
+                    sent(buf, su.at[slot, head], up)
+
+                @pl.when(jnp.logical_and(has_down, z <= plane))
+                def _(slot=slot):
+                    sent(buf, sd.at[slot, head], down)
+
+                for off in range(1, nx):
+                    sent(buf, sx.at[slot, head, off], beside[off - 1])
+        return carry
+
+    lax.fori_loop(0, kv_heads, drain, 0)
 
 
 def before(tokens):
@@ -350,7 +355,7 @@
         load.wait()
 
     def transform(dist, carry):
-        source = lax.rem(z + dist, nz)
+        source = lax.rem(z + dist + 1, nz)
         for off in range(1, count):
             j, device = plane_peer(off)
             remote(
@@ -373,7 +378,7 @@
     lax.fori_loop(0, nz, transform, 0)
 
     def combine(dist, carry):
-        source, column = column_peer(dist)
+        source, column = column_peer(dist + 1)
         for off in range(1, count):
             j, device = plane_peer(off)
             remote(
@@ -390,11 +395,11 @@
         total = (weight * (share * one + (1.0 - share) * two)).astype(BF16)
         mix[source] = total
 
-        @pl.when(dist == 0)
+        @pl.when(dist == nz - 1)
         def _():
             fin[source] = total
 
-        @pl.when(dist > 0)
+        @pl.when(dist < nz - 1)
         def _():
             remote(mix.at[source], fin.at[z], s4.at[source], t4.at[z], column).start()
 
@@ -455,17 +460,17 @@
         in_specs=[vmem] * 10 + [hbm],
         out_specs=(vmem, vmem),
         scratch_shapes=[
-            pltpu.VMEM((n_sp, tokens, kv_width), BF16),
-            pltpu.VMEM((n_sp, tokens, kv_width), BF16),
+            pltpu.VMEM((n_sp, kv_heads, tokens, HEAD_DIM), BF16),
+            pltpu.VMEM((n_sp, kv_heads, tokens, HEAD_DIM), BF16),
             pltpu.VMEM((heads, tokens, HEAD_DIM), BF16),
-            pltpu.VMEM((kv_heads, length, HEAD_DIM), BF16),
-            pltpu.VMEM((tokens, width), BF16),
-            pltpu.VMEM((tokens, width), BF16),
+            pltpu.VMEM((length, HEAD_DIM), BF16),
+            pltpu.VMEM((tokens, width // kv_heads), BF16),
+            pltpu.VMEM((tokens, width), F32),
             pltpu.VMEM((width, width), BF16),
             dma,
-            dma((n_sp,)), dma((n_sp,)),
-            dma((nx,)), dma((n_sp,)), dma((n_sp,)),
-            dma((n_sp, nx)), dma((n_sp,)), dma((n_sp,)),
+            dma((n_sp, kv_heads)), dma((n_sp, kv_heads)),
+            dma((n_sp, kv_heads, nx)), dma((n_sp, kv_heads)), dma((n_sp, kv_heads)),
+            dma((n_sp, kv_heads, nx)), dma((n_sp, kv_heads)), dma((n_sp, kv_heads)),
         ],
         compiler_params=pltpu.CompilerParams(
             collective_id=0, has_side_effects=True, vmem_limit_bytes=VMEM_LIMIT

time: 118 us -> 108 us (0.915); the launches traced: 118 us -> 106 us
  Pallas kernels: 114 us -> 102 us
    pallas_call x1, Pallas kernels: 62.1 us -> 54.8 us  [local(): pl.pallas_call(functools.partial(expert_kernel, nz, nx, n_dp), out_shape=...]
    pallas_call x1, Pallas kernels: 51.5 us -> 47.1 us  [local(): pl.pallas_call(functools.partial(attention_kernel, nz, nx), out_shape=(ro...]
where the time goes in v2:
time: 108 us; the launch traced here: 106 us
  Pallas kernels  102 us (94%)
  other arithmetic  2.01 us (2%)
  local copies, waits for them, and re-layouts  1.96 us (2%)
    pallas_call x1, Pallas kernels, local(): pl.pallas_call(functools.partial(expert_kernel, nz, nx, n_dp), out_shape=...  54.8 us
    pallas_call x1, Pallas kernels, local(): pl.pallas_call(functools.partial(attention_kernel, nz, nx), out_shape=(ro...  47.1 us

profile of v2, /device:TPU:0, one launch (start us, length us, event | category | flops | bytes accessed | tf_op | source)
XLA Modules:
  0.0 105.9 jit_solution(11307440206507037970)
XLA Ops:
  0.0 0.1 pad.3.clone
  0.1 0.7 convert_bitcast_fusion
  0.8 1.3 %maximum_maximum_fusion.meta_ref = f32[8,128]{1,0:T(8,128)} fusion(f32[1,128]{1,0:T(1,128)} %param.28, f32[1,128]{1,0:T(1,128)} %param.27, f32[2,128]{1,0:T(2,128)S(1)} %convert_bitcast_fusion, f32[8]{0:T(128)S(1)} %pad.3.clone), kind=kLoop, calls=%fused_computation | loop fusion | flops 3072 | bytes 6176 | tf_op jit(solution)/shard_map/concatenate | solution.py:491
  2.1 47.1 %attention.1 = (bf16[128,2048]{1,0:T(8,128)(2,1)}, bf16[128,2048]{1,0:T(8,128)(2,1)}) custom-call(bf16[128,2048]{1,0:T(8,128)(2,1)} %bitcast.20, bf16[128,512]{1,0:T(8,128)(2,1)} %bitcast.22, bf16[128,512]{1,0:T(8,128)(2,1)} %bitcast.23, f32[1,128]{1,0:T(1,128)} %bitcast.26, f32[1,128]{1,0:T(1,128)} %bitcast.27, f32[1024,128]{1,0:T(8,128)} %constant.6.clone.cos_ref, ...), custom_call_target="tpu_custom_call" | custom-call | tf_op jit(solution)/shard_map/attention/pallas_call | solution.py:457
  49.2 54.8 %experts.1 = bf16[128,2048]{1,0:T(8,128)(2,1)} custom-call(bf16[128,2048]{1,0:T(8,128)(2,1)} %get-tuple-element.7.normed_ref, bf16[128,2048]{1,0:T(8,128)(2,1)} %get-tuple-element.8.stream_ref, f32[8,128]{1,0:T(8,128)} %maximum_maximum_fusion.meta_ref, bf16[2048,512]{1,0:T(8,128)(2,1)} %bitcast.16, bf16[2048,512]{1,0:T(8,128)(2,1)} %bitcast.17, ...), custom_call_target="tpu_custom_call" | custom-call | tf_op jit(solution)/shard_map/experts/pallas_call | solution.py:496
  104.0 1.9 %copy.19 = bf16[1,128,2048]{2,1,0:T(8,128)(2,1)} copy(bf16[1,128,2048]{2,1,0:T(8,128)(2,1)} %bitcast.19) | data formatting | bytes 1048576
  (1 shorter events, 0.0 us)
